TPU v7x, 512 devices: a whole 4x8x8 slice. The times are simulated.
512 devices in a mesh: ep: 32 (over z, x), tp: 16 (over y, core).
Axes of the slice: x: 4, y: 8, z: 8, core: 2. Of those that a mesh axis runs over, the one named last changes fastest.
Arguments:
- tokens: bfloat16 [256, 4096], P('ep', 'tp'), may hold values from -6 to 6
- norm_gain: float32 [4096], replicated, may hold values from 0.1 to 1.9
- route_experts: int32 [256, 2], P('ep'), may hold values from 0 to 63, all different within a row; in each aligned block of 8 rows (0 to 7, 8 to 15, ...) at most 2 rows name the same one
- route_logits: float32 [256, 2], P('ep'), may hold values from -4 to 4
- expert_gate: bfloat16 [64, 4096, 1024], P('ep', None, 'tp'), may hold values from -0.09375 to 0.09375
- expert_up: bfloat16 [64, 4096, 1024], P('ep', None, 'tp'), may hold values from -0.09375 to 0.09375
- expert_down: bfloat16 [64, 1024, 4096], P('ep', 'tp'), may hold values from -0.1875 to 0.1875
- dense_gate: bfloat16 [4096, 1024], P(None, 'tp'), may hold values from -0.09375 to 0.09375
- dense_up: bfloat16 [4096, 1024], P(None, 'tp'), may hold values from -0.09375 to 0.09375
- dense_down: bfloat16 [1024, 4096], P('tp'), may hold values from -0.1875 to 0.1875
- mix_weight: float32 [4096], replicated, may hold values from -0.09375 to 0.09375
- out_gain: float32 [4096], P('tp'), may hold values from 0.1 to 1.9
Outputs:
- result: bfloat16 [256, 4096], P('ep', 'tp')
Inputs may be any that keep to these rules, and one draw needn't show every extreme that they name: `route_experts`: each row names 2 different experts; the 8 rows of one index of ep (aligned blocks) name any one expert at most 2 times, and some block names some expert exactly 2 times; every expert is named somewhere.
All inputs are finite; a program needn't handle non-finite values.
Results may differ from a plain program's by a relative error of at most 0.0025.
Values may be sent and summed in bfloat16 or wider, within the bound.
A program may use at most 64 MiB of HBM per device.

v0:
```python
import functools

import jax
import jax.numpy as jnp
from jax import lax
from jax.experimental import pallas as pl
from jax.experimental.pallas import tpu as pltpu
from jax.sharding import PartitionSpec as P

CAP = 2
CORES = 2
norm_eps = 1e-06
LOG2E = 1.4426950408889634
MESH = pl.DeviceIdType.MESH
F32 = jnp.float32
BF16 = jnp.bfloat16


def silu(v):
    return v / (1.0 + jnp.exp(-v))


def kernel(
    n_ep,
    n_tp,
    tok_hbm,
    gain_hbm,
    route_hbm,
    logit_hbm,
    eg_hbm,
    eu_hbm,
    ed_hbm,
    dg_hbm,
    du_hbm,
    dd_hbm,
    mix_hbm,
    og_hbm,
    out_ref,
    tok,
    gain,
    route,
    logit,
    eg,
    eu,
    ed,
    dg,
    du,
    dd,
    mixw,
    og,
    normed,
    placed,
    disp_send,
    disp_recv,
    rows_f,
    rows_n,
    dense_send,
    dense_recv,
    pair_send,
    pair_recv,
    summed,
    coded,
    ret_send,
    ret_recv,
    back,
    sq_send,
    sq_recv,
    lsem,
    ag_s,
    ag_r,
    di_s,
    di_r,
    fw_s,
    fw_r,
    de_s,
    de_r,
    pa_s,
    pa_r,
    re_s,
    re_r,
    sq_s,
    sq_r,
):
    me = lax.axis_index("ep")
    tp = lax.axis_index("tp")
    core = lax.rem(tp, CORES)
    row = lax.div(tp, CORES)
    n_row = n_tp // CORES
    partner = row * CORES + (1 - core)
    n_loc = eg.shape[0]
    t_rows, part = tok.shape[1], tok.shape[2]
    width = part * n_tp
    blk = n_loc * CAP
    slots = n_ep * blk

    def turn(base, d, n):
        return lax.rem(base + d, n)

    def remote(src, dst, s, r, e, t):
        return pltpu.make_async_remote_copy(
            src_ref=src,
            dst_ref=dst,
            send_sem=s,
            recv_sem=r,
            device_id={"ep": e, "tp": t},
            device_id_type=MESH,
        )

    barrier = pltpu.get_barrier_semaphore()
    greeted = 0
    for d in range(1, n_ep):
        pl.semaphore_signal(
            barrier, inc=1, device_id={"ep": turn(me, d, n_ep), "tp": tp}, device_id_type=MESH
        )
        greeted += 1
    for d in range(1, n_tp):
        pl.semaphore_signal(
            barrier, inc=1, device_id={"ep": me, "tp": turn(tp, d, n_tp)}, device_id_type=MESH
        )
        greeted += 1

    loads = []
    pairs = [
        (tok_hbm, tok.at[tp]),
        (gain_hbm, gain),
        (route_hbm, route),
        (logit_hbm, logit),
        (mix_hbm, mixw),
        (og_hbm, og),
        (dg_hbm, dg),
        (du_hbm, du),
        (dd_hbm, dd),
        (eg_hbm, eg),
        (eu_hbm, eu),
        (ed_hbm, ed),
    ]
    for i, (src, dst) in enumerate(pairs):
        c = pltpu.make_async_copy(src, dst, lsem.at[i])
        c.start()
        loads.append(c)

    near = sorted(range(1, n_ep), key=lambda d: min(d, n_ep - d))

    loads[0].wait()
    gathers = []
    for d in range(1, n_tp):
        gathers.append(
            remote(tok.at[tp], tok.at[tp], ag_s.at[d], ag_r.at[d], me, turn(tp, d, n_tp))
        )

    loads[2].wait()
    r0 = route[0:1, :]
    r1 = route[1:2, :]
    slot = lax.broadcasted_iota(jnp.int32, (slots, t_rows), 0)
    slot_e = slot // CAP
    slot_c = slot % CAP
    hit0 = (slot_e == r0).astype(F32)
    hit1 = (slot_e == r1).astype(F32)
    hits = hit0 + hit1
    ri = lax.broadcasted_iota(jnp.int32, (t_rows, t_rows), 0)
    ci = lax.broadcasted_iota(jnp.int32, (t_rows, t_rows), 1)
    before = jnp.dot(hits, (ri < ci).astype(F32), preferred_element_type=F32)
    place_t = hits * (before == slot_c.astype(F32)).astype(F32)

    placed[...] = jnp.dot(place_t.astype(BF16), tok[tp], preferred_element_type=F32)
    for p in range(n_ep):
        disp_send[p] = placed[p * blk : (p + 1) * blk, :].astype(BF16)
    for i in (1, 3, 4, 5):
        loads[i].wait()
    l0 = logit[0:1, :]
    l1 = logit[1:2, :]
    top = jnp.maximum(l0, l1)
    e0 = jnp.exp(l0 - top)
    e1 = jnp.exp(l1 - top)
    w0 = e0 / (e0 + e1)
    w1 = e1 / (e0 + e1)
    combine = (place_t * (hit0 * w0 + hit1 * w1)).T

    disp_recv[tp, me] = disp_send[me]

    pl.semaphore_wait(barrier, greeted)
    sends = {}
    for d in reversed(near):
        p = turn(me, d, n_ep)
        c = remote(disp_send.at[p], disp_recv.at[tp, me], di_s.at[d], di_r.at[d], p, tp)
        c.start()
        sends[d] = c
    for c in gathers:
        c.start()

    for d in [0] + near:
        q = turn(me, n_ep - d, n_ep)
        if d > 0:
            sends[d].wait_recv()
        for k in range(1, n_tp):
            remote(
                disp_recv.at[tp, q],
                disp_recv.at[tp, q],
                fw_s.at[k],
                fw_r.at[k],
                me,
                turn(tp, k, n_tp),
            ).start()

    for c in gathers:
        c.wait_recv()
    squares = jnp.zeros((t_rows, 1), F32)
    for t in range(n_tp):
        x = tok[t].astype(F32)
        squares += jnp.sum(x * x, axis=1, keepdims=True)
    inv = lax.rsqrt(squares / width + norm_eps)
    mix = jnp.zeros((t_rows, 1), F32)
    for t in range(n_tp):
        cols = pl.ds(t * part, part)
        nx = (tok[t].astype(F32) * inv * gain[:, cols]).astype(BF16)
        normed[:, cols] = nx
        mix += jnp.sum(nx.astype(F32) * mixw[:, cols], axis=1, keepdims=True)
    mix_gate = 1.0 / (1.0 + jnp.exp(-mix))

    for i in (6, 7):
        loads[i].wait()
    nrm = normed[...]
    dh = (
        silu(jnp.dot(nrm, dg[...], preferred_element_type=F32))
        * jnp.dot(nrm, du[...], preferred_element_type=F32)
    ).astype(BF16)
    for i in (8, 9, 10, 11):
        loads[i].wait()
    forwards = []
    for k in range(1, n_tp):
        c = remote(
            disp_recv.at[tp],
            disp_recv.at[turn(tp, n_tp - k, n_tp)],
            fw_s.at[k],
            fw_r.at[k],
            me,
            turn(tp, k, n_tp),
        )
        c.wait_recv()
        forwards.append(c)
    squares = jnp.zeros((slots, 1), F32)
    for t in range(n_tp):
        cols = pl.ds(t * part, part)
        for p in range(n_ep):
            rows_f[p * blk : (p + 1) * blk, cols] = disp_recv[t, p].astype(F32)
        x = rows_f[:, cols]
        squares += jnp.sum(x * x, axis=1, keepdims=True)
    inv = lax.rsqrt(squares / width + norm_eps)
    for t in range(n_tp):
        cols = pl.ds(t * part, part)
        rows_n[:, cols] = (rows_f[:, cols] * inv * gain[:, cols]).astype(BF16)
    x = rows_n[...]
    which = (lax.broadcasted_iota(jnp.int32, (slots, 1), 0) % blk) // CAP
    hidden = []
    for e in range(n_loc):
        h = silu(jnp.dot(x, eg[e], preferred_element_type=F32)) * jnp.dot(
            x, eu[e], preferred_element_type=F32
        )
        hidden.append(jnp.where(which == e, h, 0.0).astype(BF16))

    def down(t):
        cols = pl.ds(pl.multiple_of(t * part, 128), part)
        total = jnp.dot(hidden[0], ed[0, :, cols], preferred_element_type=F32)
        for e in range(1, n_loc):
            total += jnp.dot(hidden[e], ed[e, :, cols], preferred_element_type=F32)
        return total

    duo = []
    for y in range(n_row):
        pair_send[y] = down(y * CORES + (1 - core))
        c = remote(pair_send.at[y], pair_recv.at[y], pa_s.at[y], pa_r.at[y], me, partner)
        c.start()
        duo.append(c)
    for y in range(n_row):
        summed[y] = down(y * CORES + core)
    returns = []
    for y in range(n_row):
        duo[y].wait_recv()
        v = summed[y] + pair_recv[y]
        peak = jnp.max(jnp.abs(v), axis=1, keepdims=True)
        power = jnp.ceil(jnp.log(jnp.maximum(peak, 1e-30)) * LOG2E)
        coded[:, 0:part] = jnp.clip(
            jnp.floor(v * jnp.exp2(15.0 - power) + 0.5), -32767.0, 32767.0
        )
        coded[:, part : part + 128] = jnp.broadcast_to(power, (slots, 128))
        for p in range(n_ep):
            ret_send[y, p] = (
                coded[p * blk : (p + 1) * blk, :].astype(jnp.int32).astype(jnp.int16)
            )
    for d in range(1, n_ep):
        p = turn(me, d, n_ep)
        for k in range(n_row):
            y = turn(row, k, n_row)
            i = d * n_row + k
            c = remote(
                ret_send.at[y, p],
                ret_recv.at[row, me],
                re_s.at[i],
                re_r.at[i],
                p,
                y * CORES + core,
            )
            c.start()
            returns.append(c)
    for k in range(1, n_row):
        y = turn(row, k, n_row)
        c = remote(
            ret_send.at[y, me], ret_recv.at[row, me], re_s.at[k], re_r.at[k], me, y * CORES + core
        )
        c.start()
        returns.append(c)
    ret_recv[row, me] = ret_send[row, me]

    dense = []
    for t in range(n_tp):
        dense_send[t] = jnp.dot(
            dh, dd[:, t * part : (t + 1) * part], preferred_element_type=F32
        )
    for d in range(1, n_tp):
        t = turn(tp, d, n_tp)
        c = remote(dense_send.at[t], dense_recv.at[tp], de_s.at[d], de_r.at[d], me, t)
        c.start()
        dense.append(c)
    dense_recv[tp] = dense_send[tp]

    for c in dense:
        c.wait_recv()
    total = dense_recv[0]
    for t in range(1, n_tp):
        total += dense_recv[t]
    total = mix_gate * total
    for c in returns:
        c.wait_recv()
    mixed = jnp.zeros((slots, part), F32)
    for y in range(n_row):
        for p in range(n_ep):
            back[y, p * blk : (p + 1) * blk, :] = (
                ret_recv[y, p].astype(jnp.int32).astype(F32)
            )
        mixed += back[y, :, 0:part] * jnp.exp2(back[y, :, part : part + 1] - 15.0)
    total += jnp.dot(
        combine, mixed, preferred_element_type=F32, precision=lax.Precision.HIGHEST
    )
    sq_send[...] = jnp.broadcast_to(
        jnp.sum(total * total, axis=1, keepdims=True), sq_send.shape
    )
    swaps = []
    for d in range(1, n_tp):
        c = remote(sq_send, sq_recv.at[tp], sq_s.at[d], sq_r.at[d], me, turn(tp, d, n_tp))
        c.start()
        swaps.append(c)
    sq_recv[tp] = sq_send[...]
    for c in swaps:
        c.wait_recv()
    all_sq = sq_recv[0]
    for t in range(1, n_tp):
        all_sq += sq_recv[t]
    scale = lax.rsqrt(all_sq[:, 0:1] / width + norm_eps)
    out_ref[...] = (total * scale * og[...]).astype(out_ref.dtype)
    for c in gathers + list(sends.values()) + dense + forwards + duo + returns + swaps:
        c.wait_send()


def shards(n_ep, n_tp, *args):
    (tok, gain, route, logit, eg, eu, ed, dg, du, dd, mixw, og) = args
    t_rows, part = tok.shape
    width = part * n_tp
    n_loc, _, ff = eg.shape
    n_row = n_tp // CORES
    blk = n_loc * CAP
    slots = n_ep * blk
    dma = pltpu.SemaphoreType.DMA
    V = pltpu.VMEM
    scratch = [
        V((n_tp, t_rows, part), BF16),
        V((1, width), F32),
        V(route.shape[::-1], jnp.int32),
        V(logit.shape[::-1], F32),
        V(eg.shape, BF16),
        V(eu.shape, BF16),
        V(ed.shape, BF16),
        V(dg.shape, BF16),
        V(du.shape, BF16),
        V(dd.shape, BF16),
        V((1, width), F32),
        V((1, part), F32),
        V((t_rows, width), BF16),
        V((slots, part), F32),
        V((n_ep, blk, part), BF16),
        V((n_tp, n_ep, blk, part), BF16),
        V((slots, width), F32),
        V((slots, width), BF16),
        V((n_tp, t_rows, part), F32),
        V((n_tp, t_rows, part), F32),
        V((n_row, slots, part), F32),
        V((n_row, slots, part), F32),
        V((n_row, slots, part), F32),
        V((slots, part + 128), F32),
        V((n_row, n_ep, blk, part + 128), jnp.int16),
        V((n_row, n_ep, blk, part + 128), jnp.int16),
        V((n_row, slots, part + 128), F32),
        V((t_rows, 128), F32),
        V((n_tp, t_rows, 128), F32),
        dma((12,)),
        dma((n_tp,)),
        dma((n_tp,)),
        dma((n_ep,)),
        dma((n_ep,)),
        dma((n_tp,)),
        dma((n_tp,)),
        dma((n_tp,)),
        dma((n_tp,)),
        dma((n_row,)),
        dma((n_row,)),
        dma((n_ep * n_row,)),
        dma((n_ep * n_row,)),
        dma((n_tp,)),
        dma((n_tp,)),
    ]
    return pl.pallas_call(
        functools.partial(kernel, n_ep, n_tp),
        out_shape=jax.ShapeDtypeStruct((t_rows, part), BF16),
        in_specs=[pl.BlockSpec(memory_space=pltpu.HBM)] * 12,
        out_specs=pl.BlockSpec(memory_space=pltpu.VMEM),
        scratch_shapes=scratch,
        compiler_params=pltpu.CompilerParams(
            collective_id=0, has_side_effects=True, vmem_limit_bytes=60 * 1024 * 1024
        ),
        name="moe_layer",
    )(
        tok,
        gain.reshape(1, width),
        route.T,
        logit.T,
        eg,
        eu,
        ed,
        dg,
        du,
        dd,
        mixw.reshape(1, width),
        og.reshape(1, part),
    )


def solution(mesh):
    placed = (
        P("ep", "tp"),
        P(),
        P("ep", None),
        P("ep", None),
        P("ep", None, "tp"),
        P("ep", None, "tp"),
        P("ep", "tp", None),
        P(None, "tp"),
        P(None, "tp"),
        P("tp", None),
        P(),
        P("tp"),
    )
    return jax.shard_map(
        functools.partial(shards, mesh.shape["ep"], mesh.shape["tp"]),
        mesh=mesh,
        in_specs=placed,
        out_specs=P("ep", "tp"),
        check_vma=False,
    )
```

profile of v0, /device:TPU:1, one launch (start us, length us, event | category | flops | bytes accessed | tf_op | source)
XLA Modules:
  0.0 98.3 jit_solution(4846206977532279605)
XLA Ops:
  0.0 0.0 copy-start
  0.0 2.4 %copy.15.dg_hbm = bf16[4096,64]{1,0:T(8,128)(2,1)} copy(bf16[4096,64]{0,1:T(8,128)(2,1)} %param.19) | data formatting | bytes 1048576 | tf_op args[7]
  2.4 0.0 copy-start.1
  2.4 2.5 %copy.16.du_hbm = bf16[4096,64]{1,0:T(8,128)(2,1)} copy(bf16[4096,64]{0,1:T(8,128)(2,1)} %param.20) | data formatting | bytes 1048576 | tf_op args[8]
  4.9 0.0 copy-done
  4.9 1.8 %copy.13.eg_hbm = bf16[2,4096,64]{2,1,0:T(8,128)(2,1)} copy(bf16[2,4096,64]{1,2,0:T(8,128)(2,1)S(1)} %copy-done) | data formatting | bytes 2097152 | tf_op args[4]
  6.7 0.0 copy-done.1
  6.7 1.8 %copy.14.eu_hbm = bf16[2,4096,64]{2,1,0:T(8,128)(2,1)} copy(bf16[2,4096,64]{1,2,0:T(8,128)(2,1)S(1)} %copy-done.1) | data formatting | bytes 2097152 | tf_op args[5]
  8.5 88.5 %moe_layer.1 = bf16[8,256]{1,0:T(8,128)(2,1)} custom-call(bf16[8,256]{1,0:T(8,128)(2,1)} %tok_hbm.1, f32[1,4096]{1,0:T(1,128)} %bitcast.5, s32[2,8]{1,0:T(2,128)} %bitcast.7, f32[2,8]{1,0:T(2,128)} %bitcast.8, bf16[2,4096,64]{2,1,0:T(8,128)(2,1)} %copy.13.eg_hbm, bf16[2,4096,64]{2,1,0:T(8,128)(2,1)} %copy.14.eu_hbm, bf16[2,64,4096]{2,1,0:T(8,128)(2,1)} %ed_hbm.1, ...), custom_call_target="tpu_custom_call" | custom-call | tf_op jit(solution)/shard_map/moe_layer/pallas_call | solution.py:420
  97.0 1.3 %copy.18 = bf16[8,256]{1,0:T(8,128)(2,1)} copy(bf16[8,256]{1,0:T(8,128)(2,1)} %moe_layer.1) | data formatting | bytes 8192
Async XLA Ops:
  0.0 4.9 %copy-start = (bf16[2,4096,64]{1,2,0:T(8,128)(2,1)S(1)}, bf16[2,4096,64]{1,2,0:T(8,128)(2,1)}, u32[]{:S(2)}) copy-start(bf16[2,4096,64]{1,2,0:T(8,128)(2,1)} %param.16) | copy-start | bytes 3145732
  2.4 4.3 %copy-start.1 = (bf16[2,4096,64]{1,2,0:T(8,128)(2,1)S(1)}, bf16[2,4096,64]{1,2,0:T(8,128)(2,1)}, u32[]{:S(2)}) copy-start(bf16[2,4096,64]{1,2,0:T(8,128)(2,1)} %param.17) | copy-start | bytes 3145732
where the time goes:
time: 98.5 us; the launch traced here: 98.3 us
  Pallas kernels  88.5 us (90%)
  local copies, waits for them, and re-layouts  9.77 us (10%)
    pallas_call x1, Pallas kernels, shards(): pl.pallas_call(functools.partial(kernel, n_ep, n_tp), out_shape=jax.Shape...  88.5 us
    unnamed x9, local copies, waits for them, and re-layouts  9.77 us

commit v1 on v0

v1 whole, which is shorter than its diff:
```python
import functools

import jax
import jax.numpy as jnp
from jax import lax
from jax.experimental import pallas as pl
from jax.experimental.pallas import tpu as pltpu
from jax.sharding import PartitionSpec as P

CAP = 2
CORES = 2
NX = 4
norm_eps = 1e-06
MESH = pl.DeviceIdType.MESH
F32 = jnp.float32
BF16 = jnp.bfloat16
NT = (((1,), (1,)), ((), ()))


def silu(v):
    return v / (1.0 + jnp.exp(-v))


def far_first(i, n):
    half = (i + 1) // 2
    return n // 2 - half if i % 2 == 1 else (n // 2 + half) % n


def far_first_vec(i, n):
    half = (i + 1) >> 1
    return jnp.where((i & 1) == 1, n // 2 - half, (n // 2 + half) & (n - 1))


def kernel(
    n_ep,
    n_tp,
    n_loc,
    tok_hbm,
    gain_hbm,
    route_hbm,
    logit_hbm,
    eg_hbm,
    eu_hbm,
    ed_hbm,
    dg_hbm,
    du_hbm,
    dd_hbm,
    mix_hbm,
    og_hbm,
    out_ref,
    tok,
    gain,
    route,
    logit,
    wgu,
    ed,
    wd,
    dd,
    mixw,
    og,
    normed,
    stacked,
    disp_send,
    own_recv,
    par_recv,
    rows_n,
    hid4,
    dense_send,
    dense_recv,
    pair_send,
    pair_recv,
    ret_send,
    ret_recv,
    scl_send,
    scl_recv,
    fin_send,
    fin_recv,
    sq_send,
    sq_recv,
    lsem,
    esem,
    ag_s,
    ag_r,
    di_s,
    di_r,
    pf_s,
    pf_r,
    de_s,
    de_r,
    pa_s,
    pa_r,
    re_s,
    re_r,
    sc_s,
    sc_r,
    fi_s,
    fi_r,
    sq_s,
    sq_r,
):
    me = lax.axis_index("ep")
    tp = lax.axis_index("tp")
    core = lax.rem(tp, CORES)
    row = lax.div(tp, CORES)
    n_row = n_tp // CORES
    partner = row * CORES + (1 - core)
    t_rows, part = tok.shape[1], tok.shape[2]
    width = part * n_tp
    nx = min(NX, n_ep)
    nz = n_ep // nx
    my_z = lax.div(me, nx)
    my_x = lax.rem(me, nx)
    slot = n_loc * CAP
    nq = n_row // 2
    blk = nq * slot
    slots = n_ep * blk
    wide = 2 * part
    keys = nq * t_rows
    hid = ed.shape[1] // nq
    n_chunk = 4 if n_ep >= 8 else 2
    per = n_ep // n_chunk
    crow = per * blk
    xrow = per * slot

    def turn(base, d, n):
        return lax.rem(base + d, n)

    def remote(src, dst, s, r, e, t):
        return pltpu.make_async_remote_copy(
            src_ref=src,
            dst_ref=dst,
            send_sem=s,
            recv_sem=r,
            device_id={"ep": e, "tp": t},
            device_id_type=MESH,
        )

    def offsets(b):
        return far_first(b // nx, nz), far_first(b % nx, nx)

    def ahead(b):
        dz, dx = offsets(b)
        return turn(my_z, dz, nz) * nx + turn(my_x, dx, nx)

    def behind(b):
        dz, dx = offsets(b)
        return turn(my_z, (nz - dz) % nz, nz) * nx + turn(my_x, (nx - dx) % nx, nx)

    def natural(q, h, g):
        return CORES * (2 * q + h) + g

    barrier = pltpu.get_barrier_semaphore()
    greeted = 0
    for d in range(1, n_ep):
        pl.semaphore_signal(
            barrier, inc=1, device_id={"ep": turn(me, d, n_ep), "tp": tp}, device_id_type=MESH
        )
        greeted += 1
    for d in range(1, n_tp):
        pl.semaphore_signal(
            barrier, inc=1, device_id={"ep": me, "tp": turn(tp, d, n_tp)}, device_id_type=MESH
        )
        greeted += 1

    half_w = wgu.shape[0] // 2
    ffd = wd.shape[0] // 2
    loads = []
    pairs = [
        (tok_hbm, tok.at[tp]),
        (route_hbm, route),
        (logit_hbm, logit),
        (gain_hbm, gain),
        (mix_hbm, mixw),
        (og_hbm, og),
        (dg_hbm, wd.at[0:ffd]),
        (du_hbm, wd.at[ffd : 2 * ffd]),
        (dd_hbm, dd),
        (eg_hbm, wgu.at[0:half_w]),
        (eu_hbm, wgu.at[half_w : 2 * half_w]),
    ]
    for i, (src, dst) in enumerate(pairs):
        c = pltpu.make_async_copy(src, dst, lsem.at[i])
        c.start()
        loads.append(c)
    ed_loads = []
    for g in range(CORES):
        for q in range(nq):
            for h in range(2):
                t = natural(q, h, g)
                c = pltpu.make_async_copy(
                    ed_hbm.at[:, t * part : (t + 1) * part],
                    ed.at[g, q * hid : (q + 1) * hid, h * part : (h + 1) * part],
                    esem.at[t],
                )
                c.start()
                ed_loads.append(c)

    gathers = []
    for d in range(1, n_tp):
        gathers.append(
            remote(tok.at[tp], tok.at[tp], ag_s.at[d], ag_r.at[d], me, turn(tp, d, n_tp))
        )

    loads[1].wait()
    loads[2].wait()
    spread = (
        lax.broadcasted_iota(jnp.int32, (t_rows, keys), 0)
        == (lax.broadcasted_iota(jnp.int32, (t_rows, keys), 1) & (t_rows - 1))
    ).astype(F32)

    def tiled(v):
        return jnp.dot(v, spread, preferred_element_type=F32, precision=lax.Precision.HIGHEST)

    l0 = logit[0:1, :]
    l1 = logit[1:2, :]
    top = jnp.maximum(l0, l1)
    e0 = jnp.exp(l0 - top)
    e1 = jnp.exp(l1 - top)
    w0 = tiled(e0 / (e0 + e1))
    w1 = tiled(e1 / (e0 + e1))
    r0 = tiled(route[0:1, :].astype(F32))
    r1 = tiled(route[1:2, :].astype(F32))
    ri = lax.broadcasted_iota(jnp.int32, (keys, keys), 0)
    ci = lax.broadcasted_iota(jnp.int32, (keys, keys), 1)
    tri = ((ri < ci) & ((ri // t_rows) == (ci // t_rows))).astype(F32)
    r = lax.broadcasted_iota(jnp.int32, (slots, keys), 0)
    k = lax.broadcasted_iota(jnp.int32, (slots, keys), 1)
    b = r // blk
    s = r % slot
    dz = far_first_vec(b // nx, nz)
    dx = far_first_vec(b % nx, nx)
    dest = ((my_z + dz) & (nz - 1)) * nx + ((my_x + dx) & (nx - 1))
    slot_e = (dest * n_loc + s // CAP).astype(F32)
    same = ((r // slot) % nq) == (k // t_rows)
    hit0 = (slot_e == r0).astype(F32)
    hit1 = (slot_e == r1).astype(F32)
    hits = hit0 + hit1
    before = jnp.dot(hits, tri, preferred_element_type=F32)
    place = jnp.where(same & (before == (s % CAP).astype(F32)), hits, 0.0)
    combine = (place * (hit0 * w0 + hit1 * w1)).T
    place = place.astype(BF16)

    pr = lax.broadcasted_iota(jnp.int32, (crow, crow), 0)
    pc = lax.broadcasted_iota(jnp.int32, (crow, crow), 1)
    perm = (
        ((pr // xrow) == ((pc // slot) % nq))
        & (((pr // slot) % per) == (pc // blk))
        & ((pr % slot) == (pc % slot))
    ).astype(BF16)
    xr = lax.broadcasted_iota(jnp.int32, (crow, xrow), 0)
    xc = lax.broadcasted_iota(jnp.int32, (crow, xrow), 1)
    expand = (((xr // blk) == (xc // slot)) & ((xr % slot) == (xc % slot))).astype(BF16)
    sr = lax.broadcasted_iota(jnp.int32, (crow, 128), 0)
    scol = lax.broadcasted_iota(jnp.int32, (crow, 128), 1)
    in_lane = (sr % blk) == scol
    gr = lax.broadcasted_iota(jnp.int32, (per, crow), 0)
    gc = lax.broadcasted_iota(jnp.int32, (per, crow), 1)
    in_block = gr == (gc // blk)
    br = lax.broadcasted_iota(jnp.int32, (128, crow), 0)
    bc = lax.broadcasted_iota(jnp.int32, (128, crow), 1)
    unlane = (br == (bc % blk)).astype(BF16)

    loads[0].wait()
    pl.semaphore_wait(barrier, greeted)
    for c in gathers:
        c.start()
    loads[3].wait()
    loads[4].wait()
    loads[5].wait()
    for c in gathers:
        c.wait_recv()
    squares = jnp.zeros((t_rows, part), F32)
    for t in range(n_tp):
        x = tok[t].astype(F32)
        squares += x * x
    inv = lax.rsqrt(jnp.sum(squares, axis=1, keepdims=True) / width + norm_eps)
    for t in range(n_tp):
        cols = slice(t * part, (t + 1) * part)
        normed[:, cols] = (tok[t].astype(F32) * inv * gain[:, cols]).astype(BF16)
    for q in range(nq):
        for h in range(2):
            cols = pl.ds(pl.multiple_of(natural(q, h, core) * part, part), part)
            stacked[q * t_rows : (q + 1) * t_rows, h * part : (h + 1) * part] = normed[
                :, cols
            ].astype(F32)
    source = stacked[...].astype(BF16)
    for c in range(n_chunk):
        rows = slice(c * crow, (c + 1) * crow)
        piece = jnp.dot(place[rows, :], source, preferred_element_type=F32).astype(BF16)
        disp_send[rows, :] = piece
        for i in range(per):
            j = c * per + i
            if j < n_ep - 1:
                at = pl.ds(j * blk, blk)
                remote(
                    disp_send.at[at], own_recv.at[at], di_s, di_r.at[c], ahead(j), tp
                ).start()
    tail = slice((n_ep - 1) * blk, n_ep * blk)
    own_recv[tail, :] = disp_send[tail, :]

    mix = jnp.sum(normed[...].astype(F32) * mixw[...], axis=1, keepdims=True)
    mix_gate = 1.0 / (1.0 + jnp.exp(-mix))
    for i in (6, 7, 8):
        loads[i].wait()
    both = lax.dot_general(normed[...], wd[...], NT, preferred_element_type=F32)
    dh = (silu(both[:, 0:ffd]) * both[:, ffd : 2 * ffd]).astype(BF16)
    for t in range(n_tp):
        dense_send[t] = jnp.dot(
            dh, dd[:, t * part : (t + 1) * part], preferred_element_type=F32
        )
    dense = []
    for d in range(1, n_tp):
        t = turn(tp, d, n_tp)
        c = remote(dense_send.at[t], dense_recv.at[tp], de_s.at[d], de_r.at[d], me, t)
        c.start()
        dense.append(c)
    dense_recv[tp] = dense_send[tp]
    for i in (9, 10):
        loads[i].wait()
    for c in ed_loads:
        c.wait()

    def unpack(src, c, g):
        rows = slice(c * crow, (c + 1) * crow)
        moved = jnp.dot(perm, src[rows, :], preferred_element_type=F32).astype(BF16)
        for q in range(nq):
            for h in range(2):
                cols = pl.ds(pl.multiple_of(natural(q, h, g) * part, part), part)
                rows_n[c * xrow : (c + 1) * xrow, cols] = moved[
                    q * xrow : (q + 1) * xrow, h * part : (h + 1) * part
                ]

    forwards = []
    for c in range(n_chunk):
        n = per - (c == n_chunk - 1)
        at = pl.ds(c * crow, n * blk)
        remote(disp_send.at[at], own_recv.at[at], di_s, di_r.at[c], me, tp).wait_recv()
        at = pl.ds(c * crow, crow)
        f = remote(own_recv.at[at], par_recv.at[at], pf_s.at[c], pf_r.at[c], me, partner)
        f.start()
        forwards.append(f)
        unpack(own_recv, c, core)
    for c in range(n_chunk):
        forwards[c].wait_recv()
        unpack(par_recv, c, 1 - core)
    act = lax.dot_general(rows_n[...], wgu[...], NT, preferred_element_type=F32)
    ar = lax.broadcasted_iota(jnp.int32, (n_ep * slot, hid), 0)
    ac = lax.broadcasted_iota(jnp.int32, (n_ep * slot, hid), 1)
    mine = ((ar % slot) // CAP) == (ac // (hid // n_loc))
    hidden = jnp.where(mine, silu(act[:, 0:hid]) * act[:, hid : 2 * hid], 0.0).astype(BF16)
    hr = lax.broadcasted_iota(jnp.int32, (crow, hid), 0)
    for c in range(n_chunk):
        wider = jnp.dot(
            expand, hidden[c * xrow : (c + 1) * xrow, :], preferred_element_type=F32
        )
        for q in range(nq):
            hid4[c * crow : (c + 1) * crow, q * hid : (q + 1) * hid] = jnp.where(
                ((hr // slot) % nq) == q, wider, 0.0
            ).astype(BF16)

    duo = []
    for c in range(n_chunk):
        rows = slice(c * crow, (c + 1) * crow)
        pair_send[rows, :] = jnp.dot(hid4[rows, :], ed[1 - core], preferred_element_type=F32)
        at = pl.ds(c * crow, crow)
        f = remote(pair_send.at[at], pair_recv.at[at], pa_s.at[c], pa_r.at[c], me, partner)
        f.start()
        duo.append(f)
    for c in range(n_chunk):
        rows = slice(c * crow, (c + 1) * crow)
        v = jnp.dot(hid4[rows, :], ed[core], preferred_element_type=F32)
        duo[c].wait_recv()
        v = v + pair_recv[rows, :]
        peak = jnp.max(jnp.abs(v), axis=1, keepdims=True)
        step = (jnp.maximum(peak, 1e-30) * (1.0 / 32600.0)).astype(BF16).astype(F32)
        ret_send[rows, :] = (
            jnp.floor(v * (1.0 / step) + 0.5).astype(jnp.int32).astype(jnp.int16)
        )
        lanes = jnp.where(in_lane, step, 0.0).astype(BF16)
        steps = jnp.dot(in_block.astype(BF16), lanes, preferred_element_type=F32)
        for i in range(per):
            j = c * per + i
            scl_send[j] = steps[i : i + 1, :]
            if j < n_ep - 1:
                at = pl.ds(j * blk, blk)
                remote(
                    ret_send.at[at], ret_recv.at[at], re_s, re_r.at[c], behind(j), tp
                ).start()
                remote(
                    scl_send.at[j], scl_recv.at[j], sc_s, sc_r.at[c], behind(j), tp
                ).start()
    ret_recv[tail, :] = ret_send[tail, :]
    scl_recv[n_ep - 1] = scl_send[n_ep - 1]

    for c in dense:
        c.wait_recv()
    total = dense_recv[0]
    for t in range(1, n_tp):
        total += dense_recv[t]
    total = mix_gate * total

    mixed = jnp.zeros((keys, wide), F32)
    for c in range(n_chunk):
        n = per - (c == n_chunk - 1)
        at = pl.ds(c * crow, n * blk)
        remote(ret_send.at[at], ret_recv.at[at], re_s, re_r.at[c], me, tp).wait_recv()
        at = pl.ds(c * per, n)
        remote(scl_send.at[at], scl_recv.at[at], sc_s, sc_r.at[c], me, tp).wait_recv()
        rows = slice(c * crow, (c + 1) * crow)
        steps = jnp.concatenate([scl_recv[c * per + i] for i in range(per)], axis=0)
        lanes = jnp.dot(steps.astype(BF16), unlane, preferred_element_type=F32)
        step = jnp.sum(jnp.where(in_block, lanes, 0.0), axis=0, keepdims=True)
        back = ret_recv[rows, :].astype(jnp.int32).astype(F32)
        mixed += jnp.dot(
            combine[:, rows] * step,
            back,
            preferred_element_type=F32,
            precision=lax.Precision.HIGHEST,
        )
    for q in range(nq):
        for h in range(2):
            fin_send[2 * q + h] = mixed[
                q * t_rows : (q + 1) * t_rows, h * part : (h + 1) * part
            ]
    finals = []
    for d in range(1, n_row):
        y = turn(row, d, n_row)
        c = remote(
            fin_send.at[y], fin_recv.at[row], fi_s.at[d], fi_r.at[d], me, y * CORES + core
        )
        c.start()
        finals.append(c)
    fin_recv[row] = fin_send[row]
    for c in finals:
        c.wait_recv()
    for y in range(n_row):
        total += fin_recv[y]
    sq_send[...] = jnp.broadcast_to(
        jnp.sum(total * total, axis=1, keepdims=True), sq_send.shape
    )
    swaps = []
    for d in range(1, n_tp):
        c = remote(sq_send, sq_recv.at[tp], sq_s.at[d], sq_r.at[d], me, turn(tp, d, n_tp))
        c.start()
        swaps.append(c)
    sq_recv[tp] = sq_send[...]
    for c in swaps:
        c.wait_recv()
    all_sq = sq_recv[0]
    for t in range(1, n_tp):
        all_sq += sq_recv[t]
    scale = lax.rsqrt(all_sq[:, 0:1] / width + norm_eps)
    out_ref[...] = (total * scale * og[...]).astype(out_ref.dtype)
    for c in gathers + forwards + dense + duo + finals + swaps:
        c.wait_send()
    at = pl.ds(0, (n_ep - 1) * blk)
    remote(disp_send.at[at], own_recv.at[at], di_s, di_r.at[0], me, tp).wait_send()
    remote(ret_send.at[at], ret_recv.at[at], re_s, re_r.at[0], me, tp).wait_send()
    at = pl.ds(0, n_ep - 1)
    remote(scl_send.at[at], scl_recv.at[at], sc_s, sc_r.at[0], me, tp).wait_send()


def shards(n_ep, n_tp, *args):
    (tok, gain, route, logit, eg, eu, ed, dg, du, dd, mixw, og) = args
    t_rows, part = tok.shape
    width = part * n_tp
    n_loc, _, ff = eg.shape
    ffd = dg.shape[1]
    hid = n_loc * ff
    n_row = n_tp // CORES
    nq = n_row // 2
    slot = n_loc * CAP
    blk = nq * slot
    slots = n_ep * blk
    wide = 2 * part
    n_chunk = 4 if n_ep >= 8 else 2
    dma = pltpu.SemaphoreType.DMA
    V = pltpu.VMEM
    scratch = [
        V((n_tp, t_rows, part), BF16),
        V((1, width), F32),
        V(route.shape[::-1], jnp.int32),
        V(logit.shape[::-1], F32),
        V((2 * hid, width), BF16),
        V((CORES, nq * hid, wide), BF16),
        V((2 * ffd, width), BF16),
        V(dd.shape, BF16),
        V((1, width), F32),
        V((1, part), F32),
        V((t_rows, width), BF16),
        V((nq * t_rows, wide), F32),
        V((slots, wide), BF16),
        V((slots, wide), BF16),
        V((slots, wide), BF16),
        V((n_ep * slot, width), BF16),
        V((slots, nq * hid), BF16),
        V((n_tp, t_rows, part), F32),
        V((n_tp, t_rows, part), F32),
        V((slots, wide), F32),
        V((slots, wide), F32),
        V((slots, wide), jnp.int16),
        V((slots, wide), jnp.int16),
        V((n_ep, 1, 128), F32),
        V((n_ep, 1, 128), F32),
        V((n_row, t_rows, part), F32),
        V((n_row, t_rows, part), F32),
        V((t_rows, 128), F32),
        V((n_tp, t_rows, 128), F32),
        dma((11,)),
        dma((n_tp,)),
        dma((n_tp,)),
        dma((n_tp,)),
        dma,
        dma((n_chunk,)),
        dma((n_chunk,)),
        dma((n_chunk,)),
        dma((n_tp,)),
        dma((n_tp,)),
        dma((n_chunk,)),
        dma((n_chunk,)),
        dma,
        dma((n_chunk,)),
        dma,
        dma((n_chunk,)),
        dma((n_row,)),
        dma((n_row,)),
        dma((n_tp,)),
        dma((n_tp,)),
    ]
    return pl.pallas_call(
        functools.partial(kernel, n_ep, n_tp, n_loc),
        out_shape=jax.ShapeDtypeStruct((t_rows, part), BF16),
        in_specs=[pl.BlockSpec(memory_space=pltpu.HBM)] * 12,
        out_specs=pl.BlockSpec(memory_space=pltpu.VMEM),
        scratch_shapes=scratch,
        compiler_params=pltpu.CompilerParams(
            collective_id=0, has_side_effects=True, vmem_limit_bytes=60 * 1024 * 1024
        ),
        name="moe_layer",
    )(
        tok,
        gain.reshape(1, width),
        route.T,
        logit.T,
        eg.swapaxes(1, 2).reshape(hid, width),
        eu.swapaxes(1, 2).reshape(hid, width),
        ed.reshape(hid, width),
        dg.T,
        du.T,
        dd,
        mixw.reshape(1, width),
        og.reshape(1, part),
    )


def solution(mesh):
    placed = (
        P("ep", "tp"),
        P(),
        P("ep", None),
        P("ep", None),
        P("ep", None, "tp"),
        P("ep", None, "tp"),
        P("ep", "tp", None),
        P(None, "tp"),
        P(None, "tp"),
        P("tp", None),
        P(),
        P("tp"),
    )
    return jax.shard_map(
        functools.partial(shards, mesh.shape["ep"], mesh.shape["tp"]),
        mesh=mesh,
        in_specs=placed,
        out_specs=P("ep", "tp"),
        check_vma=False,
    )
```

time: 98.5 us -> 71.7 us (0.73)
  Pallas kernels: 88.5 us -> 70.3 us
  local copies, waits for them, and re-layouts: 9.77 us -> 1.28 us
    pallas_call x1, Pallas kernels: 88.5 us -> 70.3 us  [shards(): pl.pallas_call(functools.partial(kernel, n_ep, n_tp, n_loc), out_shape=ja...]
    unnamed x9 -> x1, local copies, waits for them, and re-layouts: 9.77 us -> 1.28 us
where the time goes in v1:
time: 71.7 us; the launch traced here: 71.6 us
  Pallas kernels  70.3 us (98%)
  local copies, waits for them, and re-layouts  1.28 us (2%)
    pallas_call x1, Pallas kernels, shards(): pl.pallas_call(functools.partial(kernel, n_ep, n_tp, n_loc), out_shape=ja...  70.3 us

profile of v1, /device:TPU:1, one launch (start us, length us, event | category | flops | bytes accessed | tf_op | source)
XLA Modules:
  0.0 71.6 jit_solution(18341553882578399621)
XLA Ops:
  0.0 70.3 %moe_layer.1 = bf16[8,256]{1,0:T(8,128)(2,1)} custom-call(bf16[8,256]{1,0:T(8,128)(2,1)} %tok_hbm.1, f32[1,4096]{1,0:T(1,128)} %bitcast.19, s32[2,8]{1,0:T(2,128)} %bitcast.21, f32[2,8]{1,0:T(2,128)} %bitcast.22, bf16[128,4096]{1,0:T(8,128)(2,1)} %bitcast.14, bf16[128,4096]{1,0:T(8,128)(2,1)} %bitcast.15, bf16[128,4096]{1,0:T(8,128)(2,1)} %bitcast.16, ...), custom_call_target="tpu_custom_call" | custom-call | tf_op jit(solution)/shard_map/moe_layer/pallas_call | solution.py:530
  70.3 1.3 %copy.14 = bf16[8,256]{1,0:T(8,128)(2,1)} copy(bf16[8,256]{1,0:T(8,128)(2,1)} %moe_layer.1) | data formatting | bytes 8192

commit v2 on v1

v2 whole, which is shorter than its diff:
```python
import functools

import jax
import jax.numpy as jnp
from jax import lax
from jax.experimental import pallas as pl
from jax.experimental.pallas import tpu as pltpu
from jax.sharding import PartitionSpec as P

CAP = 2
CORES = 2
NX = 4
CHUNKS = 4
norm_eps = 1e-06
MESH = pl.DeviceIdType.MESH
F32 = jnp.float32
BF16 = jnp.bfloat16
NT = (((1,), (1,)), ((), ()))


def silu(v):
    return v / (1.0 + jnp.exp(-v))


def chunks_of(n_ep):
    return CHUNKS if n_ep >= 2 * CHUNKS else 2


def far_first(i, n):
    half = (i + 1) // 2
    return n // 2 - half if i % 2 == 1 else (n // 2 + half) % n


def far_first_vec(i, n):
    half = (i + 1) >> 1
    return jnp.where((i & 1) == 1, n // 2 - half, (n // 2 + half) & (n - 1))


def kernel(
    n_ep,
    n_tp,
    n_loc,
    tok_hbm,
    gain_hbm,
    route_hbm,
    logit_hbm,
    eg_hbm,
    eu_hbm,
    ed_hbm,
    dg_hbm,
    du_hbm,
    dd_hbm,
    mix_hbm,
    og_hbm,
    out_ref,
    tok,
    gain,
    route,
    logit,
    wgu,
    ednat,
    ed,
    wd,
    dd,
    mixw,
    og,
    normed,
    disp_send,
    grid,
    rows_n,
    hid4,
    dense_send,
    dense_recv,
    pair_send,
    pair_recv,
    ret_send,
    ret_recv,
    scl_send,
    scl_recv,
    fin_send,
    fin_recv,
    sq_send,
    sq_recv,
    lsem,
    ag_s,
    ag_r,
    di_s,
    di_r,
    ya_s,
    ya_r,
    pf_s,
    pf_r,
    de_s,
    de_r,
    pa_s,
    pa_r,
    re_s,
    re_r,
    sc_s,
    sc_r,
    fi_s,
    fi_r,
    sq_s,
    sq_r,
):
    me = lax.axis_index("ep")
    tp = lax.axis_index("tp")
    core = lax.rem(tp, CORES)
    row = lax.div(tp, CORES)
    n_row = n_tp // CORES
    partner = row * CORES + (1 - core)
    t_rows, part = tok.shape[1], tok.shape[2]
    width = part * n_tp
    half = part // 2
    nx = min(NX, n_ep)
    nz = n_ep // nx
    my_z = lax.div(me, nx)
    my_x = lax.rem(me, nx)
    slot = n_loc * CAP
    blk = 2 * slot
    slots = n_ep * blk
    keys = 2 * t_rows
    hid = ednat.shape[0]
    n_chunk = chunks_of(n_ep)
    order = [n_chunk - 1] + list(range(n_chunk - 1))
    per = n_ep // n_chunk
    crow = per * blk
    xrow = per * slot
    nq = n_row // 2
    big = nq * slot
    brow = per * big
    wide = 2 * part
    far_rows = sorted(range(1, n_row), key=lambda d: -min(d, n_row - d))
    far_tp = sorted(range(1, n_tp), key=lambda d: -min(d, n_tp - d))

    def turn(base, d, n):
        return lax.rem(base + d, n)

    def remote(src, dst, s, r, e, t):
        return pltpu.make_async_remote_copy(
            src_ref=src,
            dst_ref=dst,
            send_sem=s,
            recv_sem=r,
            device_id={"ep": e, "tp": t},
            device_id_type=MESH,
        )

    def offsets(b):
        return far_first(b // nx, nz), far_first(b % nx, nx)

    def ahead(b):
        dz, dx = offsets(b)
        return turn(my_z, dz, nz) * nx + turn(my_x, dx, nx)

    def behind(b):
        dz, dx = offsets(b)
        return turn(my_z, (nz - dz) % nz, nz) * nx + turn(my_x, (nx - dx) % nx, nx)

    def chunk(c):
        return pl.ds(c * per, per)

    barrier = pltpu.get_barrier_semaphore()
    greeted = 0
    for j in range(n_ep - 1):
        pl.semaphore_signal(
            barrier, inc=1, device_id={"ep": ahead(j), "tp": tp}, device_id_type=MESH
        )
        greeted += 1
    for d in far_tp:
        pl.semaphore_signal(
            barrier, inc=1, device_id={"ep": me, "tp": turn(tp, d, n_tp)}, device_id_type=MESH
        )
        greeted += 1

    half_w = wgu.shape[0] // 2
    ffd = wd.shape[0] // 2
    loads = []
    pairs = [
        (tok_hbm, tok.at[tp]),
        (route_hbm, route),
        (logit_hbm, logit),
        (gain_hbm, gain),
        (mix_hbm, mixw),
        (og_hbm, og),
        (dg_hbm, wd.at[0:ffd]),
        (du_hbm, wd.at[ffd : 2 * ffd]),
        (dd_hbm, dd),
        (ed_hbm, ednat),
        (eg_hbm, wgu.at[0:half_w]),
        (eu_hbm, wgu.at[half_w : 2 * half_w]),
    ]
    for i, (src, dst) in enumerate(pairs):
        c = pltpu.make_async_copy(src, dst, lsem.at[i])
        c.start()
        loads.append(c)

    loads[1].wait()
    spread = (
        lax.broadcasted_iota(jnp.int32, (t_rows, keys), 0)
        == (lax.broadcasted_iota(jnp.int32, (t_rows, keys), 1) % t_rows)
    ).astype(F32)
    both = jnp.dot(route[...].astype(F32), spread, preferred_element_type=F32)
    ri = lax.broadcasted_iota(jnp.int32, (keys, keys), 0)
    ci = lax.broadcasted_iota(jnp.int32, (keys, keys), 1)
    tri = ((ri < ci) & ((ri // t_rows) == (ci // t_rows))).astype(F32)
    r = lax.broadcasted_iota(jnp.int32, (slots, keys), 0)
    k = lax.broadcasted_iota(jnp.int32, (slots, keys), 1)
    b = r // blk
    s = r % slot
    dz = far_first_vec(b // nx, nz)
    dx = far_first_vec(b % nx, nx)
    dest = ((my_z + dz) & (nz - 1)) * nx + ((my_x + dx) & (nx - 1))
    slot_e = (dest * n_loc + s // CAP).astype(F32)
    same = ((r // slot) % 2) == (k // t_rows)
    hit0 = (slot_e == both[0:1, :]).astype(F32)
    hit1 = (slot_e == both[1:2, :]).astype(F32)
    hits = hit0 + hit1
    before = jnp.dot(hits, tri, preferred_element_type=F32)
    place = jnp.where(same & (before == (s % CAP).astype(F32)), hits, 0.0)
    loads[0].wait()
    x = tok[tp].astype(F32)
    source = jnp.concatenate([x[:, 0:half], x[:, half:part]], axis=0).astype(BF16)
    placed = jnp.dot(place.astype(BF16), source, preferred_element_type=F32)
    placed = placed.reshape(n_ep, blk, half).astype(BF16)
    disp_send[...] = placed
    pl.semaphore_wait(barrier, greeted)
    for j in range(n_ep - 1):
        remote(
            disp_send.at[j], grid.at[core, row, j], di_s, di_r.at[j // per], ahead(j), tp
        ).start()
    for d in far_tp:
        remote(tok.at[tp], tok.at[tp], ag_s, ag_r, me, turn(tp, d, n_tp)).start()
    grid[core, row, n_ep - 1] = placed[n_ep - 1]

    loads[2].wait()
    l0 = logit[0:1, :]
    l1 = logit[1:2, :]
    top = jnp.maximum(l0, l1)
    e0 = jnp.exp(l0 - top)
    e1 = jnp.exp(l1 - top)
    shares = jnp.concatenate([e0 / (e0 + e1), e1 / (e0 + e1)], axis=0)
    names = jnp.concatenate([route[...].astype(F32), shares], axis=0)
    bkeys = nq * t_rows
    bspread = (
        lax.broadcasted_iota(jnp.int32, (t_rows, bkeys), 0)
        == (lax.broadcasted_iota(jnp.int32, (t_rows, bkeys), 1) % t_rows)
    ).astype(F32)
    names = jnp.dot(
        names, bspread, preferred_element_type=F32, precision=lax.Precision.HIGHEST
    )
    ri = lax.broadcasted_iota(jnp.int32, (bkeys, bkeys), 0)
    ci = lax.broadcasted_iota(jnp.int32, (bkeys, bkeys), 1)
    tri = ((ri < ci) & ((ri // t_rows) == (ci // t_rows))).astype(F32)
    r = lax.broadcasted_iota(jnp.int32, (n_ep * big, bkeys), 0)
    k = lax.broadcasted_iota(jnp.int32, (n_ep * big, bkeys), 1)
    b = r // big
    s = r % slot
    dz = far_first_vec(b // nx, nz)
    dx = far_first_vec(b % nx, nx)
    dest = ((my_z + dz) & (nz - 1)) * nx + ((my_x + dx) & (nx - 1))
    slot_e = (dest * n_loc + s // CAP).astype(F32)
    same = ((r // slot) % nq) == (k // t_rows)
    hit0 = (slot_e == names[0:1, :]).astype(F32)
    hit1 = (slot_e == names[1:2, :]).astype(F32)
    before = jnp.dot(hit0 + hit1, tri, preferred_element_type=F32)
    taken = same & (before == (s % CAP).astype(F32))
    combine = jnp.where(taken, hit0 * names[2:3, :] + hit1 * names[3:4, :], 0.0).T
    pr = lax.broadcasted_iota(jnp.int32, (crow, crow), 0)
    pc = lax.broadcasted_iota(jnp.int32, (crow, crow), 1)
    perm = (
        ((pr // xrow) == ((pc // slot) % 2))
        & (((pr // slot) % per) == (pc // blk))
        & ((pr % slot) == (pc % slot))
    ).astype(BF16)
    xr = lax.broadcasted_iota(jnp.int32, (brow, xrow), 0)
    xc = lax.broadcasted_iota(jnp.int32, (brow, xrow), 1)
    expand = (((xr // big) == (xc // slot)) & ((xr % slot) == (xc % slot))).astype(BF16)
    sr = lax.broadcasted_iota(jnp.int32, (brow, 128), 0)
    sc = lax.broadcasted_iota(jnp.int32, (brow, 128), 1)
    in_lane = (sr % big) == sc
    gr = lax.broadcasted_iota(jnp.int32, (per, brow), 0)
    gc = lax.broadcasted_iota(jnp.int32, (per, brow), 1)
    in_block = gr == (gc // big)
    br = lax.broadcasted_iota(jnp.int32, (128, brow), 0)
    bc = lax.broadcasted_iota(jnp.int32, (128, brow), 1)
    unlane = (br == (bc % big)).astype(BF16)
    loads[9].wait()
    for g in range(CORES):
        for q in range(nq):
            for h in range(2):
                at = (CORES * (2 * q + h) + g) * part
                ed[g, q * hid : (q + 1) * hid, h * part : (h + 1) * part] = ednat[
                    :, at : at + part
                ]

    for c in order:
        at = pl.ds(c * per, per - (c == n_chunk - 1))
        remote(
            disp_send.at[at], grid.at[core, row, at], di_s, di_r.at[c], me, tp
        ).wait_recv()
        for d in far_rows:
            spot = grid.at[core, row, chunk(c)]
            remote(spot, spot, ya_s, ya_r.at[c], me, turn(row, d, n_row) * CORES + core).start()

    for i in (3, 4, 5):
        loads[i].wait()
    at = pl.ds(0, n_tp - 1)
    remote(tok.at[at], tok.at[at], ag_s, ag_r, me, tp).wait_recv()
    squares = jnp.zeros((t_rows, part), F32)
    for t in range(n_tp):
        x = tok[t].astype(F32)
        squares += x * x
    inv = lax.rsqrt(jnp.sum(squares, axis=1, keepdims=True) / width + norm_eps)
    mix = jnp.zeros((t_rows, part), F32)
    for t in range(n_tp):
        cols = slice(t * part, (t + 1) * part)
        nt = (tok[t].astype(F32) * inv * gain[:, cols]).astype(BF16)
        normed[:, cols] = nt
        mix += nt.astype(F32) * mixw[:, cols]
    mix_gate = 1.0 / (1.0 + jnp.exp(-jnp.sum(mix, axis=1, keepdims=True)))
    for i in (6, 7, 8):
        loads[i].wait()
    both = lax.dot_general(normed[...], wd[...], NT, preferred_element_type=F32)
    dh = (silu(both[:, 0:ffd]) * both[:, ffd : 2 * ffd]).astype(BF16)
    for t in range(n_tp):
        dense_send[t] = jnp.dot(
            dh, dd[:, t * part : (t + 1) * part], preferred_element_type=F32
        )
    for d in far_tp:
        t = turn(tp, d, n_tp)
        remote(dense_send.at[t], dense_recv.at[d - 1], de_s, de_r, me, t).start()
    for i in (10, 11):
        loads[i].wait()

    def unpack(c, g):
        slabs = [
            grid[g, y, c * per : (c + 1) * per].astype(F32).reshape(crow, half)
            for y in range(n_row)
        ]
        moved = jnp.dot(
            perm, jnp.concatenate(slabs, axis=1).astype(BF16), preferred_element_type=F32
        )
        total = jnp.zeros((xrow, half), F32)
        for y in range(n_row):
            for h in range(2):
                v = moved[h * xrow : (h + 1) * xrow, y * half : (y + 1) * half]
                at = pl.multiple_of((CORES * y + g) * part + h * half, half)
                rows_n[c * xrow : (c + 1) * xrow, pl.ds(at, half)] = v.astype(BF16)
                total += v * v
        return jnp.sum(total, axis=1, keepdims=True)

    ar = lax.broadcasted_iota(jnp.int32, (xrow, hid), 0)
    ac = lax.broadcasted_iota(jnp.int32, (xrow, hid), 1)
    mine = ((ar % slot) // CAP) == (ac // (hid // n_loc))
    hr = lax.broadcasted_iota(jnp.int32, (brow, hid), 0)
    seen = {}

    def gather(c):
        at = pl.ds(0, n_row - 1)
        spot = grid.at[core, at, chunk(c)]
        remote(spot, spot, ya_s, ya_r.at[c], me, tp).wait_recv()
        spot = grid.at[core, :, chunk(c)]
        remote(spot, spot, pf_s, pf_r.at[c], me, partner).start()
        seen[c] = unpack(c, core)

    def apply(c):
        spot = grid.at[1 - core, :, chunk(c)]
        remote(spot, spot, pf_s, pf_r.at[c], me, tp).wait_recv()
        inv = lax.rsqrt((seen[c] + unpack(c, 1 - core)) / width + norm_eps)
        rows = slice(c * xrow, (c + 1) * xrow)
        for t in range(n_tp):
            cols = slice(t * part, (t + 1) * part)
            rows_n[rows, cols] = (rows_n[rows, cols].astype(F32) * inv * gain[:, cols]).astype(
                BF16
            )
        act = lax.dot_general(rows_n[rows, :], wgu[...], NT, preferred_element_type=F32)
        hidden = jnp.where(mine, silu(act[:, 0:hid]) * act[:, hid : 2 * hid], 0.0)
        wider = jnp.dot(expand, hidden.astype(BF16), preferred_element_type=F32)
        rows = slice(c * brow, (c + 1) * brow)
        for q in range(nq):
            hid4[rows, q * hid : (q + 1) * hid] = jnp.where(
                ((hr // slot) % nq) == q, wider, 0.0
            ).astype(BF16)
        pair_send[rows, :] = jnp.dot(hid4[rows, :], ed[1 - core], preferred_element_type=F32)
        at = pl.ds(c * brow, brow)
        remote(pair_send.at[at], pair_recv.at[at], pa_s, pa_r.at[c], me, partner).start()

    def reply(c):
        rows = slice(c * brow, (c + 1) * brow)
        v = jnp.dot(hid4[rows, :], ed[core], preferred_element_type=F32)
        at = pl.ds(c * brow, brow)
        remote(pair_send.at[at], pair_recv.at[at], pa_s, pa_r.at[c], me, tp).wait_recv()
        v = v + pair_recv[rows, :]
        peak = jnp.max(jnp.abs(v), axis=1, keepdims=True)
        step = (jnp.maximum(peak, 1e-30) * (1.0 / 32600.0)).astype(BF16).astype(F32)
        ret_send[rows, :] = (
            jnp.floor(v * (1.0 / step) + 0.5).astype(jnp.int32).astype(jnp.int16)
        )
        lanes = jnp.where(in_lane, step, 0.0).astype(BF16)
        steps = jnp.dot(in_block.astype(BF16), lanes, preferred_element_type=F32)
        for i in range(per):
            j = c * per + i
            scl_send[j] = steps[i : i + 1, :]
            if j < n_ep - 1:
                at = pl.ds(j * big, big)
                remote(
                    ret_send.at[at], ret_recv.at[at], re_s, re_r.at[c], behind(j), tp
                ).start()
                remote(
                    scl_send.at[j], scl_recv.at[j], sc_s, sc_r.at[c], behind(j), tp
                ).start()
        if c == n_chunk - 1:
            tail = slice((n_ep - 1) * big, n_ep * big)
            ret_recv[tail, :] = ret_send[tail, :]
            scl_recv[n_ep - 1] = scl_send[n_ep - 1]

    steps = [gather, apply, reply]
    for tick in range(n_chunk + len(steps) - 1):
        for age, step in enumerate(steps):
            if 0 <= tick - age < n_chunk:
                step(order[tick - age])
    at = pl.ds(0, n_tp - 1)
    remote(dense_recv.at[at], dense_recv.at[at], de_s, de_r, me, tp).wait_recv()
    total = dense_send[tp]
    for d in range(1, n_tp):
        total += dense_recv[d - 1]
    total = mix_gate * total
    mixed = jnp.zeros((bkeys, wide), F32)
    for c in order:
        n = per - (c == n_chunk - 1)
        at = pl.ds(c * brow, n * big)
        remote(ret_send.at[at], ret_recv.at[at], re_s, re_r.at[c], me, tp).wait_recv()
        at = pl.ds(c * per, n)
        remote(scl_send.at[at], scl_recv.at[at], sc_s, sc_r.at[c], me, tp).wait_recv()
        rows = slice(c * brow, (c + 1) * brow)
        steps = jnp.concatenate([scl_recv[c * per + i] for i in range(per)], axis=0)
        lanes = jnp.dot(steps.astype(BF16), unlane, preferred_element_type=F32)
        step = jnp.sum(jnp.where(in_block, lanes, 0.0), axis=0, keepdims=True)
        back = ret_recv[rows, :].astype(jnp.int32).astype(F32)
        mixed += jnp.dot(
            combine[:, rows] * step,
            back,
            preferred_element_type=F32,
            precision=lax.Precision.HIGHEST,
        )
    for q in range(nq):
        for h in range(2):
            fin_send[2 * q + h] = mixed[
                q * t_rows : (q + 1) * t_rows, h * part : (h + 1) * part
            ]
    for d in far_rows:
        y = turn(row, d, n_row)
        remote(
            fin_send.at[y], fin_recv.at[d - 1], fi_s, fi_r, me, y * CORES + core
        ).start()
    remote(fin_recv, fin_recv, fi_s, fi_r, me, tp).wait_recv()
    total += fin_send[row]
    for d in range(1, n_row):
        total += fin_recv[d - 1]
    eye = lax.broadcasted_iota(jnp.int32, (t_rows, 128), 0) == lax.broadcasted_iota(
        jnp.int32, (t_rows, 128), 1
    )
    mine_sq = jnp.sum(
        jnp.where(eye, jnp.sum(total * total, axis=1, keepdims=True), 0.0),
        axis=0,
        keepdims=True,
    )
    sq_send[...] = mine_sq
    for d in far_tp:
        remote(sq_send, sq_recv.at[d - 1], sq_s, sq_r, me, turn(tp, d, n_tp)).start()
    remote(sq_recv, sq_recv, sq_s, sq_r, me, tp).wait_recv()
    all_sq = mine_sq
    for d in range(1, n_tp):
        all_sq += sq_recv[d - 1]
    all_sq = jnp.sum(jnp.where(eye, all_sq, 0.0), axis=1, keepdims=True)
    scale = lax.rsqrt(all_sq / width + norm_eps)
    out_ref[...] = (total * scale * og[...]).astype(out_ref.dtype)
    at = pl.ds(0, n_tp - 1)
    remote(tok.at[at], tok.at[at], ag_s, ag_r, me, tp).wait_send()
    remote(dense_recv.at[at], dense_recv.at[at], de_s, de_r, me, tp).wait_send()
    remote(sq_recv, sq_recv, sq_s, sq_r, me, tp).wait_send()
    at = pl.ds(0, n_ep - 1)
    remote(disp_send.at[at], disp_send.at[at], di_s, di_r.at[0], me, tp).wait_send()
    remote(scl_send.at[at], scl_recv.at[at], sc_s, sc_r.at[0], me, tp).wait_send()
    at = pl.ds(0, (n_ep - 1) * big)
    remote(ret_send.at[at], ret_recv.at[at], re_s, re_r.at[0], me, tp).wait_send()
    spot = grid.at[0, pl.ds(0, n_row - 1)]
    remote(spot, spot, ya_s, ya_r.at[0], me, tp).wait_send()
    remote(grid.at[0], grid.at[0], pf_s, pf_r.at[0], me, tp).wait_send()
    remote(pair_send, pair_recv, pa_s, pa_r.at[0], me, tp).wait_send()
    remote(fin_recv, fin_recv, fi_s, fi_r, me, tp).wait_send()


def shards(n_ep, n_tp, *args):
    (tok, gain, route, logit, eg, eu, ed, dg, du, dd, mixw, og) = args
    t_rows, part = tok.shape
    width = part * n_tp
    half = part // 2
    n_loc, _, ff = eg.shape
    ffd = dg.shape[1]
    hid = n_loc * ff
    n_row = n_tp // CORES
    slot = n_loc * CAP
    blk = 2 * slot
    nq = n_row // 2
    big = n_ep * nq * slot
    wide = 2 * part
    n_chunk = chunks_of(n_ep)
    dma = pltpu.SemaphoreType.DMA
    V = pltpu.VMEM
    scratch = [
        V((n_tp, t_rows, part), BF16),
        V((1, width), F32),
        V(route.shape[::-1], jnp.int32),
        V(logit.shape[::-1], F32),
        V((2 * hid, width), BF16),
        V((hid, width), BF16),
        V((CORES, nq * hid, wide), BF16),
        V((2 * ffd, width), BF16),
        V(dd.shape, BF16),
        V((1, width), F32),
        V((1, part), F32),
        V((t_rows, width), BF16),
        V((n_ep, blk, half), BF16),
        V((CORES, n_row, n_ep, blk, half), BF16),
        V((n_ep * slot, width), BF16),
        V((big, nq * hid), BF16),
        V((n_tp, t_rows, part), F32),
        V((n_tp - 1, t_rows, part), F32),
        V((big, wide), F32),
        V((big, wide), F32),
        V((big, wide), jnp.int16),
        V((big, wide), jnp.int16),
        V((n_ep, 1, 128), F32),
        V((n_ep, 1, 128), F32),
        V((n_row, t_rows, part), F32),
        V((n_row - 1, t_rows, part), F32),
        V((1, 128), F32),
        V((n_tp - 1, 1, 128), F32),
        dma((12,)),
        dma,
        dma,
        dma,
        dma((n_chunk,)),
        dma,
        dma((n_chunk,)),
        dma,
        dma((n_chunk,)),
        dma,
        dma,
        dma,
        dma((n_chunk,)),
        dma,
        dma((n_chunk,)),
        dma,
        dma((n_chunk,)),
        dma,
        dma,
        dma,
        dma,
    ]
    return pl.pallas_call(
        functools.partial(kernel, n_ep, n_tp, n_loc),
        out_shape=jax.ShapeDtypeStruct((t_rows, part), BF16),
        in_specs=[pl.BlockSpec(memory_space=pltpu.HBM)] * 12,
        out_specs=pl.BlockSpec(memory_space=pltpu.VMEM),
        scratch_shapes=scratch,
        compiler_params=pltpu.CompilerParams(
            collective_id=0, has_side_effects=True, vmem_limit_bytes=60 * 1024 * 1024
        ),
        name="moe_layer",
    )(
        tok,
        gain.reshape(1, width),
        route.T,
        logit.T,
        eg.swapaxes(1, 2).reshape(hid, width),
        eu.swapaxes(1, 2).reshape(hid, width),
        ed.reshape(hid, width),
        dg.T,
        du.T,
        dd,
        mixw.reshape(1, width),
        og.reshape(1, part),
    )


def solution(mesh):
    placed = (
        P("ep", "tp"),
        P(),
        P("ep", None),
        P("ep", None),
        P("ep", None, "tp"),
        P("ep", None, "tp"),
        P("ep", "tp", None),
        P(None, "tp"),
        P(None, "tp"),
        P("tp", None),
        P(),
        P("tp"),
    )
    return jax.shard_map(
        functools.partial(shards, mesh.shape["ep"], mesh.shape["tp"]),
        mesh=mesh,
        in_specs=placed,
        out_specs=P("ep", "tp"),
        check_vma=False,
    )
```

time: 71.7 us -> 65 us (0.907)
  Pallas kernels: 70.3 us -> 63.6 us
    pallas_call x1, Pallas kernels: 70.3 us -> 63.6 us  [shards(): pl.pallas_call(functools.partial(kernel, n_ep, n_tp, n_loc), out_shape=ja...]
where the time goes in v2:
time: 65 us; the launch traced here: 64.8 us
  Pallas kernels  63.6 us (98%)
  local copies, waits for them, and re-layouts  1.28 us (2%)
    pallas_call x1, Pallas kernels, shards(): pl.pallas_call(functools.partial(kernel, n_ep, n_tp, n_loc), out_shape=ja...  63.6 us

profile of v2, /device:TPU:1, one launch (start us, length us, event | category | flops | bytes accessed | tf_op | source)
XLA Modules:
  0.0 64.8 jit_solution(4349811737536258860)
XLA Ops:
  0.0 63.6 %moe_layer.1 = bf16[8,256]{1,0:T(8,128)(2,1)} custom-call(bf16[8,256]{1,0:T(8,128)(2,1)} %tok_hbm.1, f32[1,4096]{1,0:T(1,128)} %bitcast.19, s32[2,8]{1,0:T(2,128)} %bitcast.21, f32[2,8]{1,0:T(2,128)} %bitcast.22, bf16[128,4096]{1,0:T(8,128)(2,1)} %bitcast.14, bf16[128,4096]{1,0:T(8,128)(2,1)} %bitcast.15, bf16[128,4096]{1,0:T(8,128)(2,1)} %bitcast.16, ...), custom_call_target="tpu_custom_call" | custom-call | tf_op jit(solution)/shard_map/moe_layer/pallas_call | solution.py:563
  63.6 1.3 %copy.14 = bf16[8,256]{1,0:T(8,128)(2,1)} copy(bf16[8,256]{1,0:T(8,128)(2,1)} %moe_layer.1) | data formatting | bytes 8192

commit v3 on v2

--- a/solution.py
+++ b/solution.py
@@ -26,14 +26,20 @@
     return CHUNKS if n_ep >= 2 * CHUNKS else 2
 
 
-def far_first(i, n):
-    half = (i + 1) // 2
-    return n // 2 - half if i % 2 == 1 else (n // 2 + half) % n
-
-
-def far_first_vec(i, n):
-    half = (i + 1) >> 1
-    return jnp.where((i & 1) == 1, n // 2 - half, (n // 2 + half) & (n - 1))
+def paired(i, n):
+    h = n // 2 - 1 - i // 2
+    if i < n - 2:
+        return h if i % 2 == 0 else n - h
+    return n // 2 if i == n - 2 else 0
+
+
+def paired_vec(i, n):
+    h = n // 2 - 1 - (i >> 1)
+    return jnp.where(
+        i < n - 2,
+        jnp.where((i & 1) == 0, h, n - h),
+        jnp.where(i == n - 2, n // 2, 0),
+    )
 
 
 def kernel(
@@ -122,7 +128,7 @@
     keys = 2 * t_rows
     hid = ednat.shape[0]
     n_chunk = chunks_of(n_ep)
-    order = [n_chunk - 1] + list(range(n_chunk - 1))
+    order = [0, 3, 1, 2]
     per = n_ep // n_chunk
     crow = per * blk
     xrow = per * slot
@@ -147,7 +153,7 @@
         )
 
     def offsets(b):
-        return far_first(b // nx, nz), far_first(b % nx, nx)
+        return paired(b // nx, nz), paired(b % nx, nx)
 
     def ahead(b):
         dz, dx = offsets(b)
@@ -159,19 +165,6 @@
 
     def chunk(c):
         return pl.ds(c * per, per)
-
-    barrier = pltpu.get_barrier_semaphore()
-    greeted = 0
-    for j in range(n_ep - 1):
-        pl.semaphore_signal(
-            barrier, inc=1, device_id={"ep": ahead(j), "tp": tp}, device_id_type=MESH
-        )
-        greeted += 1
-    for d in far_tp:
-        pl.semaphore_signal(
-            barrier, inc=1, device_id={"ep": me, "tp": turn(tp, d, n_tp)}, device_id_type=MESH
-        )
-        greeted += 1
 
     half_w = wgu.shape[0] // 2
     ffd = wd.shape[0] // 2
@@ -191,9 +184,23 @@
         (eu_hbm, wgu.at[half_w : 2 * half_w]),
     ]
     for i, (src, dst) in enumerate(pairs):
-        c = pltpu.make_async_copy(src, dst, lsem.at[i])
+        loads.append(pltpu.make_async_copy(src, dst, lsem.at[i]))
+    for c in loads[0:2]:
         c.start()
-        loads.append(c)
+    barrier = pltpu.get_barrier_semaphore()
+    greeted = 0
+    for j in range(n_ep - 1):
+        pl.semaphore_signal(
+            barrier, inc=1, device_id={"ep": ahead(j), "tp": tp}, device_id_type=MESH
+        )
+        greeted += 1
+    for d in far_tp:
+        pl.semaphore_signal(
+            barrier, inc=1, device_id={"ep": me, "tp": turn(tp, d, n_tp)}, device_id_type=MESH
+        )
+        greeted += 1
+    for c in loads[2:]:
+        c.start()
 
     loads[1].wait()
     spread = (
@@ -208,8 +215,8 @@
     k = lax.broadcasted_iota(jnp.int32, (slots, keys), 1)
     b = r // blk
     s = r % slot
-    dz = far_first_vec(b // nx, nz)
-    dx = far_first_vec(b % nx, nx)
+    dz = paired_vec(b // nx, nz)
+    dx = paired_vec(b % nx, nx)
     dest = ((my_z + dz) & (nz - 1)) * nx + ((my_x + dx) & (nx - 1))
     slot_e = (dest * n_loc + s // CAP).astype(F32)
     same = ((r // slot) % 2) == (k // t_rows)
@@ -256,8 +263,8 @@
     k = lax.broadcasted_iota(jnp.int32, (n_ep * big, bkeys), 1)
     b = r // big
     s = r % slot
-    dz = far_first_vec(b // nx, nz)
-    dx = far_first_vec(b % nx, nx)
+    dz = paired_vec(b // nx, nz)
+    dx = paired_vec(b % nx, nx)
     dest = ((my_z + dz) & (nz - 1)) * nx + ((my_x + dx) & (nx - 1))
     slot_e = (dest * n_loc + s // CAP).astype(F32)
     same = ((r // slot) % nq) == (k // t_rows)
@@ -415,11 +422,12 @@
             ret_recv[tail, :] = ret_send[tail, :]
             scl_recv[n_ep - 1] = scl_send[n_ep - 1]
 
-    steps = [gather, apply, reply]
-    for tick in range(n_chunk + len(steps) - 1):
-        for age, step in enumerate(steps):
-            if 0 <= tick - age < n_chunk:
-                step(order[tick - age])
+    for i, c in enumerate(order):
+        gather(c)
+        if i > 0:
+            reply(order[i - 1])
+        apply(c)
+    reply(order[-1])
     at = pl.ds(0, n_tp - 1)
     remote(dense_recv.at[at], dense_recv.at[at], de_s, de_r, me, tp).wait_recv()
     total = dense_send[tp]

time: 65 us -> 63.1 us (0.971)
  Pallas kernels: 63.6 us -> 61.6 us
    pallas_call x1, Pallas kernels: 63.6 us -> 61.6 us  [shards(): pl.pallas_call(functools.partial(kernel, n_ep, n_tp, n_loc), out_shape=ja...]
where the time goes in v3:
time: 63.1 us; the launch traced here: 62.9 us
  Pallas kernels  61.6 us (98%)
  local copies, waits for them, and re-layouts  1.28 us (2%)
    pallas_call x1, Pallas kernels, shards(): pl.pallas_call(functools.partial(kernel, n_ep, n_tp, n_loc), out_shape=ja...  61.6 us
    unnamed x1, local copies, waits for them, and re-layouts  1.28 us

profile of v3, /device:TPU:1, one launch (start us, length us, event | category | flops | bytes accessed | tf_op | source)
XLA Modules:
  0.0 62.9 jit_solution(6503148568875002113)
XLA Ops:
  0.0 61.6 %moe_layer.1 = bf16[8,256]{1,0:T(8,128)(2,1)} custom-call(bf16[8,256]{1,0:T(8,128)(2,1)} %tok_hbm.1, f32[1,4096]{1,0:T(1,128)} %bitcast.19, s32[2,8]{1,0:T(2,128)} %bitcast.21, f32[2,8]{1,0:T(2,128)} %bitcast.22, bf16[128,4096]{1,0:T(8,128)(2,1)} %bitcast.14, bf16[128,4096]{1,0:T(8,128)(2,1)} %bitcast.15, bf16[128,4096]{1,0:T(8,128)(2,1)} %bitcast.16, ...), custom_call_target="tpu_custom_call" | custom-call | tf_op jit(solution)/shard_map/moe_layer/pallas_call | solution.py:571
  61.6 1.3 %copy.14 = bf16[8,256]{1,0:T(8,128)(2,1)} copy(bf16[8,256]{1,0:T(8,128)(2,1)} %moe_layer.1) | data formatting | bytes 8192

commit v4 on v3

--- a/solution.py
+++ b/solution.py
@@ -410,24 +410,36 @@
             j = c * per + i
             scl_send[j] = steps[i : i + 1, :]
             if j < n_ep - 1:
+                remote(
+                    scl_send.at[j], scl_recv.at[j], sc_s, sc_r.at[c], behind(j), tp
+                ).start()
+        for i in range(per):
+            j = c * per + i
+            if j < n_ep - 1:
                 at = pl.ds(j * big, big)
                 remote(
                     ret_send.at[at], ret_recv.at[at], re_s, re_r.at[c], behind(j), tp
-                ).start()
-                remote(
-                    scl_send.at[j], scl_recv.at[j], sc_s, sc_r.at[c], behind(j), tp
                 ).start()
         if c == n_chunk - 1:
             tail = slice((n_ep - 1) * big, n_ep * big)
             ret_recv[tail, :] = ret_send[tail, :]
             scl_recv[n_ep - 1] = scl_send[n_ep - 1]
 
-    for i, c in enumerate(order):
-        gather(c)
-        if i > 0:
-            reply(order[i - 1])
-        apply(c)
-    reply(order[-1])
+    for run, i in (
+        (gather, 0),
+        (apply, 0),
+        (gather, 1),
+        (reply, 0),
+        (apply, 1),
+        (gather, 2),
+        (reply, 1),
+        (gather, 3),
+        (apply, 2),
+        (apply, 3),
+        (reply, 2),
+        (reply, 3),
+    ):
+        run(order[i])
     at = pl.ds(0, n_tp - 1)
     remote(dense_recv.at[at], dense_recv.at[at], de_s, de_r, me, tp).wait_recv()
     total = dense_send[tp]

time: 63.1 us -> 61.8 us (0.979)
  Pallas kernels: 61.6 us -> 60.4 us
    pallas_call x1, Pallas kernels: 61.6 us -> 60.4 us  [shards(): pl.pallas_call(functools.partial(kernel, n_ep, n_tp, n_loc), out_shape=ja...]
where the time goes in v4:
time: 61.8 us; the launch traced here: 61.6 us
  Pallas kernels  60.4 us (98%)
  local copies, waits for them, and re-layouts  1.28 us (2%)
    pallas_call x1, Pallas kernels, shards(): pl.pallas_call(functools.partial(kernel, n_ep, n_tp, n_loc), out_shape=ja...  60.4 us
    unnamed x1, local copies, waits for them, and re-layouts  1.28 us

profile of v4, /device:TPU:1, one launch (start us, length us, event | category | flops | bytes accessed | tf_op | source)
XLA Modules:
  0.0 61.6 jit_solution(15356368198181811566)
XLA Ops:
  0.0 60.4 %moe_layer.1 = bf16[8,256]{1,0:T(8,128)(2,1)} custom-call(bf16[8,256]{1,0:T(8,128)(2,1)} %tok_hbm.1, f32[1,4096]{1,0:T(1,128)} %bitcast.19, s32[2,8]{1,0:T(2,128)} %bitcast.21, f32[2,8]{1,0:T(2,128)} %bitcast.22, bf16[128,4096]{1,0:T(8,128)(2,1)} %bitcast.14, bf16[128,4096]{1,0:T(8,128)(2,1)} %bitcast.15, bf16[128,4096]{1,0:T(8,128)(2,1)} %bitcast.16, ...), custom_call_target="tpu_custom_call" | custom-call | tf_op jit(solution)/shard_map/moe_layer/pallas_call | solution.py:583
  60.4 1.3 %copy.14 = bf16[8,256]{1,0:T(8,128)(2,1)} copy(bf16[8,256]{1,0:T(8,128)(2,1)} %moe_layer.1) | data formatting | bytes 8192

commit v5 on v4

--- a/solution.py
+++ b/solution.py
@@ -120,6 +120,7 @@
     half = part // 2
     nx = min(NX, n_ep)
     nz = n_ep // nx
+    both_ways = min(2, nz)
     my_z = lax.div(me, nx)
     my_x = lax.rem(me, nx)
     slot = n_loc * CAP
@@ -153,7 +154,8 @@
         )
 
     def offsets(b):
-        return paired(b // nx, nz), paired(b % nx, nx)
+        iz = both_ways * (b // (both_ways * nx)) + b % both_ways
+        return paired(iz, nz), paired(b % (both_ways * nx) // both_ways, nx)
 
     def ahead(b):
         dz, dx = offsets(b)
@@ -215,8 +217,8 @@
     k = lax.broadcasted_iota(jnp.int32, (slots, keys), 1)
     b = r // blk
     s = r % slot
-    dz = paired_vec(b // nx, nz)
-    dx = paired_vec(b % nx, nx)
+    dz = paired_vec(both_ways * (b // (both_ways * nx)) + b % both_ways, nz)
+    dx = paired_vec((b % (both_ways * nx)) // both_ways, nx)
     dest = ((my_z + dz) & (nz - 1)) * nx + ((my_x + dx) & (nx - 1))
     slot_e = (dest * n_loc + s // CAP).astype(F32)
     same = ((r // slot) % 2) == (k // t_rows)
@@ -263,8 +265,8 @@
     k = lax.broadcasted_iota(jnp.int32, (n_ep * big, bkeys), 1)
     b = r // big
     s = r % slot
-    dz = paired_vec(b // nx, nz)
-    dx = paired_vec(b % nx, nx)
+    dz = paired_vec(both_ways * (b // (both_ways * nx)) + b % both_ways, nz)
+    dx = paired_vec((b % (both_ways * nx)) // both_ways, nx)
     dest = ((my_z + dz) & (nz - 1)) * nx + ((my_x + dx) & (nx - 1))
     slot_e = (dest * n_loc + s // CAP).astype(F32)
     same = ((r // slot) % nq) == (k // t_rows)

time: 61.8 us -> 61.5 us (level)
  no operation moved by 1% of the time
where the time goes in v5:
time: 61.5 us; the launch traced here: 61.3 us
  Pallas kernels  60.1 us (98%)
  local copies, waits for them, and re-layouts  1.28 us (2%)
    pallas_call x1, Pallas kernels, shards(): pl.pallas_call(functools.partial(kernel, n_ep, n_tp, n_loc), out_shape=ja...  60.1 us
    unnamed x1, local copies, waits for them, and re-layouts  1.28 us

profile of v5, /device:TPU:1, one launch (start us, length us, event | category | flops | bytes accessed | tf_op | source)
XLA Modules:
  0.0 61.3 jit_solution(6816882470949590492)
XLA Ops:
  0.0 60.1 %moe_layer.1 = bf16[8,256]{1,0:T(8,128)(2,1)} custom-call(bf16[8,256]{1,0:T(8,128)(2,1)} %tok_hbm.1, f32[1,4096]{1,0:T(1,128)} %bitcast.19, s32[2,8]{1,0:T(2,128)} %bitcast.21, f32[2,8]{1,0:T(2,128)} %bitcast.22, bf16[128,4096]{1,0:T(8,128)(2,1)} %bitcast.14, bf16[128,4096]{1,0:T(8,128)(2,1)} %bitcast.15, bf16[128,4096]{1,0:T(8,128)(2,1)} %bitcast.16, ...), custom_call_target="tpu_custom_call" | custom-call | tf_op jit(solution)/shard_map/moe_layer/pallas_call | solution.py:585
  60.1 1.3 %copy.14 = bf16[8,256]{1,0:T(8,128)(2,1)} copy(bf16[8,256]{1,0:T(8,128)(2,1)} %moe_layer.1) | data formatting | bytes 8192

commit v6 on v5

--- a/solution.py
+++ b/solution.py
@@ -403,9 +403,6 @@
         v = v + pair_recv[rows, :]
         peak = jnp.max(jnp.abs(v), axis=1, keepdims=True)
         step = (jnp.maximum(peak, 1e-30) * (1.0 / 32600.0)).astype(BF16).astype(F32)
-        ret_send[rows, :] = (
-            jnp.floor(v * (1.0 / step) + 0.5).astype(jnp.int32).astype(jnp.int16)
-        )
         lanes = jnp.where(in_lane, step, 0.0).astype(BF16)
         steps = jnp.dot(in_block.astype(BF16), lanes, preferred_element_type=F32)
         for i in range(per):
@@ -415,6 +412,9 @@
                 remote(
                     scl_send.at[j], scl_recv.at[j], sc_s, sc_r.at[c], behind(j), tp
                 ).start()
+        ret_send[rows, :] = (
+            jnp.floor(v * (1.0 / step) + 0.5).astype(jnp.int32).astype(jnp.int16)
+        )
         for i in range(per):
             j = c * per + i
             if j < n_ep - 1:

time: 61.5 us -> 62.4 us (1.015)
  Pallas kernels: 60.1 us -> 61 us
    pallas_call x1, Pallas kernels: 60.1 us -> 61 us  [shards(): pl.pallas_call(functools.partial(kernel, n_ep, n_tp, n_loc), out_shape=ja...]
where the time goes in v6:
time: 62.4 us; the launch traced here: 62.2 us
  Pallas kernels  61 us (98%)
  local copies, waits for them, and re-layouts  1.28 us (2%)
    pallas_call x1, Pallas kernels, shards(): pl.pallas_call(functools.partial(kernel, n_ep, n_tp, n_loc), out_shape=ja...  61 us
    unnamed x1, local copies, waits for them, and re-layouts  1.28 us

profile of v6, /device:TPU:1, one launch (start us, length us, event | category | flops | bytes accessed | tf_op | source)
XLA Modules:
  0.0 62.2 jit_solution(13289928975646751656)
XLA Ops:
  0.0 61.0 %moe_layer.1 = bf16[8,256]{1,0:T(8,128)(2,1)} custom-call(bf16[8,256]{1,0:T(8,128)(2,1)} %tok_hbm.1, f32[1,4096]{1,0:T(1,128)} %bitcast.19, s32[2,8]{1,0:T(2,128)} %bitcast.21, f32[2,8]{1,0:T(2,128)} %bitcast.22, bf16[128,4096]{1,0:T(8,128)(2,1)} %bitcast.14, bf16[128,4096]{1,0:T(8,128)(2,1)} %bitcast.15, bf16[128,4096]{1,0:T(8,128)(2,1)} %bitcast.16, ...), custom_call_target="tpu_custom_call" | custom-call | tf_op jit(solution)/shard_map/moe_layer/pallas_call | solution.py:585
  61.0 1.3 %copy.14 = bf16[8,256]{1,0:T(8,128)(2,1)} copy(bf16[8,256]{1,0:T(8,128)(2,1)} %moe_layer.1) | data formatting | bytes 8192
